TPU v7x, 32 devices: a whole 2x2x4 slice. The times are simulated.
32 devices in a mesh: sp: 8 (over z, core), tp: 4 (over y, x).
Axes of the slice: x: 2, y: 2, z: 4, core: 2. Of those that a mesh axis runs over, the one named last changes fastest.
Arguments:
- queries: bfloat16 [4096, 1024], P('sp', 'tp'), may hold values from -20 to 20
- key_vectors: bfloat16 [4096, 1024], P('sp', 'tp'), may hold values from -20 to 20
- value_vectors: bfloat16 [4096, 1024], P('sp', 'tp'), may hold values from -6 to 6
- log_gate_sums: float32 [4096, 16], P('sp', 'tp'), may hold values from -588 to 0, as said below
- residual: bfloat16 [4096, 2048], P('sp', 'tp'), may hold values from -24 to 24
- out_weight: bfloat16 [1024, 2048], P(None, 'tp'), may hold values from -0.75 to 0.75
- norm_gain: bfloat16 [2048], replicated, may hold values from 0.099609375 to 1.8984375
- routes: int32 [4096, 2], P('sp'), may hold values from 0 to 31, all different within a row; in each aligned block of 512 rows (0 to 511, 512 to 1023, ...) at most 40 rows name the same one
- route_weight: float32 [4096, 2], P('sp'), may hold values from 0.5 to 1.5
- expert_gate: bfloat16 [32, 2048, 512], P('sp', None, 'tp'), may hold values from -0.125 to 0.125
- expert_up: bfloat16 [32, 2048, 512], P('sp', None, 'tp'), may hold values from -0.125 to 0.125
- expert_down: bfloat16 [32, 512, 2048], P('sp', None, 'tp'), may hold values from -0.25 to 0.25
- shared_gate: bfloat16 [2048, 512], P(None, 'tp'), may hold values from -0.125 to 0.125
- shared_up: bfloat16 [2048, 512], P(None, 'tp'), may hold values from -0.125 to 0.125
- shared_down: bfloat16 [512, 2048], P(None, 'tp'), may hold values from -0.25 to 0.25
Outputs:
- layer_out: bfloat16 [4096, 2048], P('sp', 'tp')
Inputs may be any that keep to these rules, and one draw needn't show every extreme that they name: `log_gate_sums`: for each head the values do not rise along the positions. `routes`: each row names 2 different experts; among the rows of one index of sp no expert is named by more than 40 rows, a bound that some block reaches.
All inputs are finite; a program needn't handle non-finite values.
Results may differ from a plain program's by a relative error of at most 0.014.
Values may be sent and summed in bfloat16 or wider, within the bound.
A program may use at most 64 MiB of HBM per device.

v0:
```python
import math
import jax
import jax.numpy as jnp
from jax import lax
from jax.sharding import PartitionSpec as P

HDIM = 64
EPSILON = 1e-06


def silu_gate(gate_part, up_part):
    return jax.nn.silu(gate_part) * up_part


def slot_targets(routes, experts_all, capacity):
    flat_routes = routes.reshape(-1)
    onehot = (flat_routes[:, None] == jnp.arange(experts_all, dtype=jnp.int32)[None, :]).astype(
        jnp.int32
    )
    before = jnp.cumsum(onehot, axis=0) - onehot
    return flat_routes * capacity + jnp.sum(before * onehot, axis=1)


def keep_state(fold_state):
    return fold_state


def shards(
    queries,
    key_vectors,
    value_vectors,
    log_gate_sums,
    residual,
    out_weight,
    norm_gain,
    routes,
    route_weight,
    expert_gate,
    expert_up,
    expert_down,
    shared_gate,
    shared_up,
    shared_down,
):
    tok_dev = queries.shape[0]
    head_dim = HDIM
    local_heads = log_gate_sums.shape[1]
    local_width = residual.shape[1]
    model_width = norm_gain.shape[0]
    score_scale = head_dim ** (-0.5)
    seq_first = lax.axis_index("sp") * tok_dev
    query_heads = queries.reshape(tok_dev, local_heads, head_dim)
    query_pos = seq_first + jnp.arange(tok_dev, dtype=jnp.int32)
    own_gates = log_gate_sums.T
    all_gates = lax.all_gather(log_gate_sums, "sp", axis=0, tiled=True)
    initial = (
        jnp.full((local_heads, tok_dev), -1e30, jnp.float32),
        jnp.zeros((local_heads, tok_dev), jnp.float32),
        jnp.zeros((local_heads, tok_dev, head_dim), jnp.float32),
    )
    key_heads = key_vectors.reshape(tok_dev, local_heads, head_dim)
    value_heads = value_vectors.reshape(tok_dev, local_heads, head_dim)
    key_part = lax.all_gather(key_heads, "sp", axis=0, tiled=True)
    value_part = lax.all_gather(value_heads, "sp", axis=0, tiled=True)
    part_rows = key_part.shape[0]
    block_size = math.gcd(part_rows, 512)
    key_blocks = key_part.reshape(part_rows // block_size, block_size, local_heads, head_dim)
    value_blocks = value_part.reshape(part_rows // block_size, block_size, local_heads, head_dim)

    def one_block(fold_state, inputs):
        key_block, value_block, block_number = inputs
        block_first = block_number * block_size

        def compute(old_state):
            running_max, weight_total, summed = old_state
            gate_block = lax.dynamic_slice_in_dim(all_gates, block_first, block_size, 0).T
            scores = (
                jnp.einsum(
                    "qhd,khd->hqk", query_heads, key_block, preferred_element_type=jnp.float32
                )
                * score_scale
            )
            scores = scores + own_gates[:, :, None] - gate_block[:, None, :]
            key_pos = block_first + jnp.arange(block_size, dtype=jnp.int32)
            allowed = (key_pos[None, :] <= query_pos[:, None])[None]
            newmax = jnp.maximum(running_max, jnp.max(jnp.where(allowed, scores, -jnp.inf), axis=2))
            factor = jnp.exp(running_max - newmax)
            weight = jnp.where(allowed, jnp.exp(scores - newmax[:, :, None]), 0.0)
            weight_total = weight_total * factor + jnp.sum(weight, axis=2)
            summed = summed * factor[:, :, None] + jnp.einsum(
                "hqk,khd->hqd",
                weight.astype(jnp.bfloat16),
                value_block,
                preferred_element_type=jnp.float32,
            )
            return (newmax, weight_total, summed)

        useful = block_first <= seq_first + tok_dev - 1
        return (lax.cond(useful, compute, keep_state, fold_state), None)

    numbers = jnp.arange(part_rows // block_size, dtype=jnp.int32)
    result_state, _ = lax.scan(one_block, initial, (key_blocks, value_blocks, numbers))
    running_max, weight_total, summed = result_state
    attended = (summed / weight_total[:, :, None]).astype(jnp.bfloat16)
    attended = attended.transpose(1, 0, 2).reshape(tok_dev, local_heads * head_dim)
    weight_rows = out_weight
    projected = jnp.dot(
        lax.all_gather(attended, "tp", axis=1, tiled=True),
        weight_rows,
        preferred_element_type=jnp.float32,
    )
    mid = (residual.astype(jnp.float32) + projected).astype(jnp.bfloat16)
    mid_wide = mid.astype(jnp.float32)
    feature_first = lax.axis_index("tp") * local_width
    squares = lax.psum(jnp.sum(mid_wide * mid_wide, axis=1), "tp")
    inverse = lax.rsqrt(squares / model_width + EPSILON)
    own_gain = lax.dynamic_slice_in_dim(norm_gain, feature_first, local_width, 0).astype(
        jnp.float32
    )
    normed_own = (mid_wide * inverse[:, None] * own_gain[None, :]).astype(jnp.bfloat16)
    normed = lax.all_gather(normed_own, "tp", axis=1, tiled=True)
    shared_mid = silu_gate(
        jnp.dot(normed, shared_gate, preferred_element_type=jnp.float32),
        jnp.dot(normed, shared_up, preferred_element_type=jnp.float32),
    ).astype(jnp.bfloat16)
    weight_rows = shared_down
    shared_out = jnp.dot(
        lax.all_gather(shared_mid, "tp", axis=1, tiled=True),
        weight_rows,
        preferred_element_type=jnp.float32,
    )
    exp_dev = expert_gate.shape[0]
    sp_count = lax.axis_size("sp")
    experts_all = exp_dev * sp_count
    top_count = routes.shape[1]
    capacity = 5 * tok_dev * top_count // (4 * experts_all)
    targets = slot_targets(routes, experts_all, capacity)
    owners = (
        jnp.full((experts_all * capacity,), tok_dev, jnp.int32)
        .at[targets]
        .set(jnp.arange(tok_dev * top_count, dtype=jnp.int32) // top_count)
    )
    padded = jnp.concatenate(
        [normed_own, jnp.zeros((1, normed_own.shape[1]), jnp.bfloat16)], axis=0
    )
    outgoing = padded[owners].reshape(sp_count, exp_dev, capacity, normed_own.shape[1])
    rows_all = lax.all_gather(
        lax.all_to_all(outgoing, "sp", split_axis=0, concat_axis=0, tiled=True),
        "tp",
        axis=3,
        tiled=True,
    )
    gate_part = jnp.einsum(
        "secd,edf->secf", rows_all, expert_gate, preferred_element_type=jnp.float32
    )
    up_part = jnp.einsum("secd,edf->secf", rows_all, expert_up, preferred_element_type=jnp.float32)
    hidden = silu_gate(gate_part, up_part).astype(jnp.bfloat16)
    hidden_all = lax.all_gather(hidden, "tp", axis=3, tiled=True)
    produced = jnp.einsum(
        "secf,efd->secd", hidden_all, expert_down, preferred_element_type=jnp.float32
    ).astype(jnp.bfloat16)
    returned = lax.all_to_all(produced, "sp", split_axis=0, concat_axis=0, tiled=True)
    returned_flat = returned.reshape(experts_all * capacity, local_width)
    picked = returned_flat[targets].astype(jnp.float32).reshape(tok_dev, top_count, local_width)
    routed = jnp.sum(picked * route_weight[:, :, None], axis=1)
    return (mid_wide + shared_out + routed).astype(jnp.bfloat16)


def solution(mesh):
    placed = (
        P("sp", "tp"),
        P("sp", "tp"),
        P("sp", "tp"),
        P("sp", "tp"),
        P("sp", "tp"),
        P(None, "tp"),
        P(),
        P("sp", None),
        P("sp", None),
        P("sp", None, "tp"),
        P("sp", None, "tp"),
        P("sp", None, "tp"),
        P(None, "tp"),
        P(None, "tp"),
        P(None, "tp"),
    )
    return jax.shard_map(
        shards, mesh=mesh, in_specs=placed, out_specs=P("sp", "tp"), check_vma=False
    )
```

profile of v0, /device:TPU:0, one launch (start us, length us, event | category | flops | bytes accessed | tf_op | source)
XLA Modules:
  0.0 383.8 jit_solution(4985606902853403032)
XLA Ops:
  6.5 1.9 copy.36
  8.6 1.8 copy.34
  11.8 15.9 %all_gather.25 = f32[4096,4]{0,1:T(4,128)S(1)} all-gather(f32[512,4]{0,1:T(4,128)S(1)} %copy-done.9), channel_id=1, replica_groups=mesh['sp'=8,'tp'=4] {'sp'}, dimensions={0}, use_global_device_ids=true | all-gather | bytes 73728 | tf_op jit(solution)/shard_map/all_gather | solution.py:55
  27.7 13.3 %all-gather.9.cloned.1.call-done = bf16[4096,4,64]{0,2,1:T(8,128)(2,1)} async-done(((bf16[512,4,64]{0,2,1:T(8,128)(2,1)}), bf16[4096,4,64]{0,2,1:T(8,128)(2,1)}) %all-gather.9.cloned.1.call-update) | async-done | bytes 2097168 | tf_op jit(solution)/shard_map/all_gather | solution.py:64
  41.0 3.2 copy.57
  44.2 27.0 %all-gather.7.cloned.1.call-done = bf16[4096,4,64]{0,2,1:T(8,128)(2,1)} async-done(((bf16[512,4,64]{0,2,1:T(8,128)(2,1)}), bf16[4096,4,64]{0,2,1:T(8,128)(2,1)}) %all-gather.7.cloned.1.call-update) | async-done | bytes 2097168 | tf_op jit(solution)/shard_map/all_gather | solution.py:63
  71.3 3.2 copy.58
  74.6 16.6 %while.17 = (s32[]{:T(128)}, f32[4,512]{1,0:T(4,128)S(1)}, f32[4,512]{1,0:T(4,128)S(1)}, f32[4,512,64]{1,2,0:T(8,128)S(1)}, s32[8]{0:T(128)S(1)}, /*index=5*/s32...) while((s32[]{:T(128)}, f32[4,512]{1,0:T(4,128)S(1)}, ...), condition=%wide.region_5.6_spmd.clone, body=%wide.region_0.5_spmd.clone.sunk | while | flops 286790656 | bytes 15676785 | solution.py:102
  75.8 6.3 %conditional.3 = ((f32[4,512]{1,0:T(4,128)S(1)}, f32[4,512]{1,0:T(4,128)S(1)}, f32[4,512,64]{1,2,0:T(8,128)S(1)})) conditional(s32[]{:T(128)} %convert_element_type.105, (f32[4,512]{1,0:T(4,128)S(1)}, f32[4,512]{1,0:T(4,128)S(1)}, f32[4,512,64]{1,2,0:T(8,128)S(1)}) %tuple.50, (s32[]{:T(128)}, s32[]{:T(128)}, bf16[8,512,4,64]{1,3,2,0:T(8,128)(2,1)}, ...), branch_computations={%region_1.1_spmd, %region_2.4_spmd} | conditional | flops 286790656 | bytes 15674446 | solution.py:99
  76.2 2.2 fusion.2
  78.4 1.4 fusion.6
  79.8 2.3 fusion.10
  92.0 9.0 %reduce-window.6 = s32[32,8,128]{2,1,0:T(8,128)S(1)} reduce-window(s32[32,8,128]{2,1,0:T(8,128)S(1)} %fusion.56, s32[]{:T(128)} %constant.93.clone.1), window={size=1x1x128 pad=0_0x0_0x127_0}, to_apply=%region_8.9 | reduce-window | flops 4161536 | bytes 262148 | tf_op jit(solution)/shard_map/reduce-window
  101.9 4.3 %scatter_custom_fusion = s32[1280]{0:T(1024)S(1)} fusion(s32[1024]{0:T(1024)S(1)} %bitcast.129, s32[1024]{0:T(1024)S(1)} %add_select_fusion, s32[]{:T(128)} %constant.98.clone.1), kind=kCustom, calls=%fused_computation.75 | custom fusion | bytes 5124 | tf_op jit(solution)/shard_map/scatter | solution.py:141
  107.0 54.9 %all-gather.11.cloned.1.call-done = bf16[512,1024]{0,1:T(8,128)(2,1)} async-done(((bf16[512,256]{0,1:T(8,128)(2,1)}), bf16[512,1024]{0,1:T(8,128)(2,1)}) %all-gather.11.cloned.1.call-update) | async-done | bytes 1048592 | tf_op jit(solution)/shard_map/all_gather | solution.py:108
  161.9 2.5 fusion.50
  164.4 8.9 %psum.7 = f32[512]{0:T(512)S(1)} all-reduce(f32[512]{0:T(512)S(1)} %get-tuple-element.335), channel_id=1, replica_groups=mesh['sp'=8,'tp'=4] {'tp'}, use_global_device_ids=true, to_apply=%region_7.8 | all-reduce | flops 512 | bytes 4096 | tf_op jit(solution)/shard_map/psum | solution.py:115
  173.6 4.7 %gather_fusion = bf16[1280,512]{1,0:T(8,128)(2,1)} fusion(bf16[513,512]{1,0:T(8,128)(2,1)S(1)} %concatenate.3, s32[2048]{0:T(1024)S(1)} %pad_clamp_fusion), kind=kCustom, calls=%fused_computation | custom fusion | bytes 2626560 | tf_op jit(solution)/shard_map/gather | solution.py:146
  178.4 36.8 %all_to_all.10 = bf16[8,4,40,512]{3,2,1,0:T(8,128)(2,1)S(1)} all-to-all(bf16[8,4,40,512]{3,2,1,0:T(8,128)(2,1)} %bitcast.116), channel_id=1, replica_groups=mesh['sp'=8,'tp'=4] {'sp'}, dimensions={0} | all-to-all | bytes 2621440 | tf_op jit(solution)/shard_map/all_to_all | solution.py:148
  216.6 59.0 %all-gather.15.cloned.1.call-done = bf16[8,4,40,2048]{3,2,0,1:T(8,128)(2,1)} async-done(((bf16[8,4,40,512]{3,2,0,1:T(8,128)(2,1)}), bf16[8,4,40,2048]{3,2,0,1:T(8,128)(2,1)}) %all-gather.15.cloned.1.call-update) | async-done | bytes 5242896 | tf_op jit(solution)/shard_map/all_gather | solution.py:147
  275.7 4.8 %fusion.37 = f32[8,4,40,128]{3,2,0,1:T(8,128)S(1)} fusion(bf16[8,4,40,2048]{3,2,0,1:T(8,128)(2,1)} %all-gather.15.cloned.1.call-done, bf16[4,2048,128]{2,1,0:T(8,128)(2,1)} %param.28), kind=kOutput, calls=%fused_computation.48 | convolution fusion | flops 671088640 | bytes 7995392 | tf_op jit(solution)/shard_map/secd,edf->secf/dot_general | solution.py:153
  281.0 2.3 fusion.46
  283.9 28.1 %all-gather.17.cloned.1.call-done = bf16[8,4,40,512]{3,2,0,1:T(8,128)(2,1)} async-done(((bf16[8,4,40,128]{3,2,0,1:T(8,128)(2,1)}), bf16[8,4,40,512]{3,2,0,1:T(8,128)(2,1)}) %all-gather.17.cloned.1.call-update) | async-done | bytes 1310736 | tf_op jit(solution)/shard_map/all_gather | solution.py:158
  312.0 2.2 fusion.31
  315.3 4.6 %all-to-all-start.1 = ((bf16[8,4,40,512]{3,2,1,0:T(8,128)(2,1)}), bf16[8,4,40,512]{3,2,1,0:T(8,128)(2,1)S(1)}, u32[]{:S(2)}, u32[]{:S(2)}) async-start(bf16[8,4,40,512]{3,2,1,0:T(8,128)(2,1)} %copy.45), calls=%async_computation.1 | async-start | bytes 2621440 | tf_op jit(solution)/shard_map/all_to_all | solution.py:162
  320.8 27.9 %all-gather.13.cloned.1.call-done = bf16[512,2048]{1,0:T(8,128)(2,1)} async-done(((bf16[512,512]{1,0:T(8,128)(2,1)}), bf16[512,2048]{1,0:T(8,128)(2,1)}) %all-gather.13.cloned.1.call-update) | async-done | bytes 2097168 | tf_op jit(solution)/shard_map/all_gather | solution.py:121
  348.7 2.5 fusion.62
  352.0 10.6 %all_gather.29 = bf16[512,512]{1,0:T(8,128)(2,1)} all-gather(bf16[512,128]{1,0:T(8,128)(2,1)S(1)} %fusion.49), channel_id=1, replica_groups=mesh['sp'=8,'tp'=4] {'tp'}, dimensions={1}, use_global_device_ids=true | all-gather | bytes 655360 | tf_op jit(solution)/shard_map/all_gather | solution.py:128
  362.6 5.1 %gather_fusion.1 = bf16[1024,512]{1,0:T(8,128)(2,1)} fusion(bf16[1280,512]{1,0:T(8,128)(2,1)S(1)} %bitcast.115, s32[1024]{0:T(1024)S(1)} %broadcast_clamp_fusion), kind=kCustom, calls=%fused_computation.1 | custom fusion | bytes 2101248 | tf_op jit(solution)/shard_map/gather | solution.py:164
  367.7 3.4 reshape.124
  371.1 4.5 %multiply_reduce_fusion = f32[512,512]{1,0:T(8,128)S(1)} fusion(f32[512,2,512]{2,1,0:T(2,128)} %reshape.124, f32[512,2]{1,0:T(8,128)S(1)} %copy-done.7), kind=kLoop, calls=%fused_computation.38 | loop fusion | flops 786432 | bytes 3149824 | tf_op jit(solution)/shard_map/reduce_sum | solution.py:165
  375.7 1.2 fusion.36
  (105 shorter events, 14.6 us)
Async XLA Ops:
  6.5 305.4 %copy-start = (bf16[4,512,512]{2,1,0:T(8,128)(2,1)S(1)}, bf16[4,512,512]{2,1,0:T(8,128)(2,1)}, u32[]{:S(2)}) copy-start(bf16[4,512,512]{2,1,0:T(8,128)(2,1)} %param.30) | copy-start | bytes 6291460
  6.5 5.1 %copy-start.10 = (bf16[512,256]{1,0:T(8,128)(2,1)S(1)}, bf16[512,256]{1,0:T(8,128)(2,1)}, u32[]{:S(2)}) copy-start(bf16[512,256]{1,0:T(8,128)(2,1)} %param.19) | copy-start | bytes 786436
  6.5 5.2 %copy-start.9 = (f32[512,4]{0,1:T(4,128)S(1)}, f32[512,4]{0,1:T(4,128)}, u32[]{:S(2)}) copy-start(f32[512,4]{0,1:T(4,128)} %param.22) | copy-start | bytes 24580
  6.5 34.5 %all-gather.9.cloned.1.call-start = ((), (), s32[]{:S(2)}) async-start(), calls=%async_computation.3 | async-start | bytes 2359296 | tf_op jit(solution)/shard_map/all_gather | solution.py:64
  8.5 62.8 %all-gather.7.cloned.1.call-start = ((), (), s32[]{:S(2)}) async-start(), calls=%async_computation.2 | async-start | bytes 2359296 | tf_op jit(solution)/shard_map/all_gather | solution.py:63
  10.4 151.5 %all-gather.11.cloned.1.call-start = ((), (), s32[]{:S(2)}) async-start(), calls=%async_computation.4 | async-start | bytes 1310720 | tf_op jit(solution)/shard_map/all_gather | solution.py:108
  74.6 26.8 %copy-start.11 = (s32[512,2]{0,1:T(2,128)S(1)}, s32[512,2]{0,1:T(2,128)}, u32[]{:S(2)}) copy-start(s32[512,2]{0,1:T(2,128)} %param.26) | copy-start | bytes 12292
  92.0 183.7 %all-gather.15.cloned.1.call-start = ((), (), s32[]{:S(2)}) async-start(), calls=%async_computation.6 | async-start | bytes 6553600 | tf_op jit(solution)/shard_map/all_gather | solution.py:147
  164.4 9.2 %copy-start.5 = (bf16[512,512]{1,0:T(8,128)(2,1)}, bf16[512,512]{1,0:T(8,128)(2,1)S(1)}, u32[]{:S(2)}) copy-start(bf16[512,512]{1,0:T(8,128)(2,1)S(1)} %get-tuple-element.336) | copy-start | bytes 1572868
  173.6 4.8 %copy-start.2 = (bf16[512,512]{1,0:T(8,128)(2,1)}, bf16[512,512]{1,0:T(8,128)(2,1)S(1)}, u32[]{:S(2)}) copy-start(bf16[512,512]{1,0:T(8,128)(2,1)S(1)} %fusion.52) | copy-start | bytes 1572868
  216.4 95.6 %all-gather.17.cloned.1.call-start = ((), (), s32[]{:S(2)}) async-start(), calls=%async_computation.7 | async-start | bytes 1638400 | tf_op jit(solution)/shard_map/all_gather | solution.py:158
  275.7 4.8 %copy-start.1 = (bf16[8,4,40,2048]{3,2,0,1:T(8,128)(2,1)S(1)}, bf16[8,4,40,2048]{3,2,0,1:T(8,128)(2,1)}, u32[]{:S(2)}) copy-start(bf16[8,4,40,2048]{3,2,0,1:T(8,128)(2,1)} %all-gather.15.cloned.1.call-done) | copy-start | bytes 15728644
  275.7 5.3 %copy-start.13 = (bf16[4,2048,128]{2,1,0:T(8,128)(2,1)S(1)}, bf16[4,2048,128]{2,1,0:T(8,128)(2,1)}, u32[]{:S(2)}) copy-start(bf16[4,2048,128]{2,1,0:T(8,128)(2,1)} %param.29) | copy-start | bytes 6291460
  283.3 65.4 %all-gather.13.cloned.1.call-start = ((), (), s32[]{:S(2)}) async-start(), calls=%async_computation.5 | async-start | bytes 2621440 | tf_op jit(solution)/shard_map/all_gather | solution.py:121
  314.1 5.8 %copy-start.12 = (f32[512,2]{0,1:T(2,128)S(1)}, f32[512,2]{0,1:T(2,128)}, u32[]{:S(2)}) copy-start(f32[512,2]{0,1:T(2,128)} %param.27) | copy-start | bytes 12292
  315.3 47.3 %all-to-all-start.1 = ((bf16[8,4,40,512]{3,2,1,0:T(8,128)(2,1)}), bf16[8,4,40,512]{3,2,1,0:T(8,128)(2,1)S(1)}, u32[]{:S(2)}, u32[]{:S(2)}) async-start(bf16[8,4,40,512]{3,2,1,0:T(8,128)(2,1)} %copy.45), calls=%async_computation.1 | async-start | bytes 2621440 | tf_op jit(solution)/shard_map/all_to_all | solution.py:162
  348.7 2.5 copy-start.3
  348.7 2.5 copy-start.14
  367.7 3.4 copy-start.7
  371.1 4.5 %copy-start.4 = (bf16[512,512]{1,0:T(8,128)(2,1)S(1)}, bf16[512,512]{1,0:T(8,128)(2,1)}, u32[]{:S(2)}) copy-start(bf16[512,512]{1,0:T(8,128)(2,1)} %all_gather.29) | copy-start | bytes 1572868
  371.1 4.5 %copy-start.6 = (bf16[512,512]{1,0:T(8,128)(2,1)S(1)}, bf16[512,512]{1,0:T(8,128)(2,1)}, u32[]{:S(2)}) copy-start(bf16[512,512]{1,0:T(8,128)(2,1)} %copy-done.5) | copy-start | bytes 1572868
  371.1 4.6 %copy-start.8 = (bf16[512,512]{1,0:T(8,128)(2,1)S(1)}, bf16[512,512]{1,0:T(8,128)(2,1)}, u32[]{:S(2)}) copy-start(bf16[512,512]{1,0:T(8,128)(2,1)} %param.33) | copy-start | bytes 1572868
Sparse Core Ops, SparseCore 0:
  8.9 32.0 all-gather.8
  42.6 28.6 all-gather.6
  92.1 69.7 all-gather.10
  216.5 59.1 all-gather.14
  283.4 28.5 all-gather.16
  313.6 35.0 all-gather.12
where the time goes:
time: 385 us; the launch traced here: 384 us
  waiting for transfers between devices  211 us (55%)
  blocking collectives  72.3 us (19%)
  local copies, waits for them, and re-layouts  38.3 us (10%)
  matrix products  20.8 us (5%)
  other arithmetic  17.1 us (4%)
  between operations  13.8 us (4%)
  loops' own time  5.65 us (1%)
  starting transfers between devices  4.99 us (1%)
    all_gather x1, waiting for transfers between devices, shards(): lax.all_gather(lax.all_to_all(outgoing, 'sp', split_axis=0, concat_axis=0...  59 us
    all_gather x1, waiting for transfers between devices, shards(): lax.all_gather(attended, 'tp', axis=1, tiled=True)  54.9 us
    all_to_all x1, blocking collectives, shards(): lax.all_to_all(outgoing, 'sp', split_axis=0, concat_axis=0, tiled=True)  36.8 us
    all_gather x1, waiting for transfers between devices, shards(): hidden_all = lax.all_gather(hidden, 'tp', axis=3, tiled=True)  28.1 us
    all_gather x1, waiting for transfers between devices, shards(): normed = lax.all_gather(normed_own, 'tp', axis=1, tiled=True)  27.9 us
    all_gather x1, waiting for transfers between devices, shards(): key_part = lax.all_gather(key_heads, 'sp', axis=0, tiled=True)  27 us
    all_gather x1, blocking collectives, shards(): all_gates = lax.all_gather(log_gate_sums, 'sp', axis=0, tiled=True)  15.9 us
    all_gather x1, waiting for transfers between devices, shards(): value_part = lax.all_gather(value_heads, 'sp', axis=0, tiled=True)  13.3 us
  transfers between devices with their start and end apart: 7, of which 6 were waited for; matrix products, arithmetic and copies ran while one was open for 7% of the time, Pallas kernels for 0%

commit v1 on v0

--- a/solution.py
+++ b/solution.py
@@ -105,7 +105,7 @@
     attended = attended.transpose(1, 0, 2).reshape(tok_dev, local_heads * head_dim)
     weight_rows = out_weight
     projected = jnp.dot(
-        lax.all_gather(attended, "tp", axis=1, tiled=True),
+        jnp.concatenate(lax.all_gather(attended, axis_name="tp"), axis=1),
         weight_rows,
         preferred_element_type=jnp.float32,
     )

time: 385 us -> 387 us (level)
  no operation moved by 1% of the time
where the time goes in v1:
time: 387 us; the launch traced here: 386 us
  waiting for transfers between devices  211 us (55%)
  blocking collectives  72.3 us (19%)
  local copies, waits for them, and re-layouts  41.4 us (11%)
  matrix products  20.8 us (5%)
  other arithmetic  16.4 us (4%)
  between operations  13.8 us (4%)
  loops' own time  5.65 us (1%)
  starting transfers between devices  4.99 us (1%)
    all_gather x1, waiting for transfers between devices, shards(): lax.all_gather(lax.all_to_all(outgoing, 'sp', split_axis=0, concat_axis=0...  59 us
    all_gather x1, waiting for transfers between devices, shards(): lax.all_gather(attended, axis_name='tp')  54.8 us
    all_to_all x1, blocking collectives, shards(): lax.all_to_all(outgoing, 'sp', split_axis=0, concat_axis=0, tiled=True)  36.8 us
    all_gather x1, waiting for transfers between devices, shards(): hidden_all = lax.all_gather(hidden, 'tp', axis=3, tiled=True)  28.1 us
    all_gather x1, waiting for transfers between devices, shards(): normed = lax.all_gather(normed_own, 'tp', axis=1, tiled=True)  27.9 us
    all_gather x1, waiting for transfers between devices, shards(): key_part = lax.all_gather(key_heads, 'sp', axis=0, tiled=True)  27 us
    all_gather x1, blocking collectives, shards(): all_gates = lax.all_gather(log_gate_sums, 'sp', axis=0, tiled=True)  15.9 us
    all_gather x1, waiting for transfers between devices, shards(): value_part = lax.all_gather(value_heads, 'sp', axis=0, tiled=True)  13.3 us
  transfers between devices with their start and end apart: 7, of which 6 were waited for; matrix products, arithmetic and copies ran while one was open for 7% of the time, Pallas kernels for 0%

profile of v1, /device:TPU:0, one launch (start us, length us, event | category | flops | bytes accessed | tf_op | source)
XLA Modules:
  0.0 386.1 jit_solution(5567132486718074868)
XLA Ops:
  6.5 1.9 copy.51
  8.6 1.8 copy.49
  11.8 15.9 %all_gather.25 = f32[4096,4]{0,1:T(4,128)S(1)} all-gather(f32[512,4]{0,1:T(4,128)S(1)} %copy-done.9), channel_id=1, replica_groups=mesh['sp'=8,'tp'=4] {'sp'}, dimensions={0}, use_global_device_ids=true | all-gather | bytes 73728 | tf_op jit(solution)/shard_map/all_gather | solution.py:55
  27.7 13.3 %all-gather.9.cloned.1.call-done = bf16[4096,4,64]{0,2,1:T(8,128)(2,1)} async-done(((bf16[512,4,64]{0,2,1:T(8,128)(2,1)}), bf16[4096,4,64]{0,2,1:T(8,128)(2,1)}) %all-gather.9.cloned.1.call-update) | async-done | bytes 2097168 | tf_op jit(solution)/shard_map/all_gather | solution.py:64
  41.0 3.2 copy.74
  44.2 27.0 %all-gather.7.cloned.1.call-done = bf16[4096,4,64]{0,2,1:T(8,128)(2,1)} async-done(((bf16[512,4,64]{0,2,1:T(8,128)(2,1)}), bf16[4096,4,64]{0,2,1:T(8,128)(2,1)}) %all-gather.7.cloned.1.call-update) | async-done | bytes 2097168 | tf_op jit(solution)/shard_map/all_gather | solution.py:63
  71.3 3.2 copy.75
  74.6 16.6 %while.17 = (s32[]{:T(128)}, f32[4,512]{1,0:T(4,128)S(1)}, f32[4,512]{1,0:T(4,128)S(1)}, f32[4,512,64]{1,2,0:T(8,128)S(1)}, s32[8]{0:T(128)S(1)}, /*index=5*/s32...) while((s32[]{:T(128)}, f32[4,512]{1,0:T(4,128)S(1)}, ...), condition=%wide.region_5.6_spmd.clone, body=%wide.region_0.5_spmd.clone.sunk | while | flops 286790656 | bytes 15676785 | solution.py:102
  75.8 6.3 %conditional.3 = ((f32[4,512]{1,0:T(4,128)S(1)}, f32[4,512]{1,0:T(4,128)S(1)}, f32[4,512,64]{1,2,0:T(8,128)S(1)})) conditional(s32[]{:T(128)} %convert_element_type.105, (f32[4,512]{1,0:T(4,128)S(1)}, f32[4,512]{1,0:T(4,128)S(1)}, f32[4,512,64]{1,2,0:T(8,128)S(1)}) %tuple.51, (s32[]{:T(128)}, s32[]{:T(128)}, bf16[8,512,4,64]{1,3,2,0:T(8,128)(2,1)}, ...), branch_computations={%region_1.1_spmd, %region_2.4_spmd} | conditional | flops 286790656 | bytes 15674446 | solution.py:99
  76.2 2.2 fusion.2
  78.4 1.4 fusion.6
  79.8 2.3 fusion.10
  92.2 9.0 %reduce-window.6 = s32[32,8,128]{2,1,0:T(8,128)S(1)} reduce-window(s32[32,8,128]{2,1,0:T(8,128)S(1)} %fusion.56, s32[]{:T(128)} %constant.93.clone.1), window={size=1x1x128 pad=0_0x0_0x127_0}, to_apply=%region_8.9 | reduce-window | flops 4161536 | bytes 262148 | tf_op jit(solution)/shard_map/reduce-window
  102.1 4.3 %scatter_custom_fusion = s32[1280]{0:T(1024)S(1)} fusion(s32[1024]{0:T(1024)S(1)} %bitcast.133, s32[1024]{0:T(1024)S(1)} %add_select_fusion, s32[]{:T(128)} %constant.98.clone.1), kind=kCustom, calls=%fused_computation.75 | custom fusion | bytes 5124 | tf_op jit(solution)/shard_map/scatter | solution.py:141
  107.2 54.8 %all-gather.11.cloned.1.call-done = bf16[4,512,256]{2,1,0:T(8,128)(2,1)} async-done(((bf16[1,512,256]{2,1,0:T(8,128)(2,1)}), bf16[4,512,256]{2,1,0:T(8,128)(2,1)}) %all-gather.11.cloned.1.call-update) | async-done | bytes 1048592 | tf_op jit(solution)/shard_map/all_gather | solution.py:108
  162.0 2.3 copy.55
  164.3 2.5 fusion.50
  166.8 8.9 %psum.7 = f32[512]{0:T(512)S(1)} all-reduce(f32[512]{0:T(512)S(1)} %get-tuple-element.347), channel_id=1, replica_groups=mesh['sp'=8,'tp'=4] {'tp'}, use_global_device_ids=true, to_apply=%region_7.8 | all-reduce | flops 512 | bytes 4096 | tf_op jit(solution)/shard_map/psum | solution.py:115
  176.0 4.7 %gather_fusion = bf16[1280,512]{1,0:T(8,128)(2,1)} fusion(bf16[513,512]{1,0:T(8,128)(2,1)S(1)} %concatenate.3, s32[2048]{0:T(1024)S(1)} %pad_clamp_fusion), kind=kCustom, calls=%fused_computation | custom fusion | bytes 2626560 | tf_op jit(solution)/shard_map/gather | solution.py:146
  180.8 36.8 %all_to_all.10 = bf16[8,4,40,512]{3,2,1,0:T(8,128)(2,1)S(1)} all-to-all(bf16[8,4,40,512]{3,2,1,0:T(8,128)(2,1)} %bitcast.119), channel_id=1, replica_groups=mesh['sp'=8,'tp'=4] {'sp'}, dimensions={0} | all-to-all | bytes 2621440 | tf_op jit(solution)/shard_map/all_to_all | solution.py:148
  219.0 59.0 %all-gather.15.cloned.1.call-done = bf16[8,4,40,2048]{3,2,0,1:T(8,128)(2,1)} async-done(((bf16[8,4,40,512]{3,2,0,1:T(8,128)(2,1)}), bf16[8,4,40,2048]{3,2,0,1:T(8,128)(2,1)}) %all-gather.15.cloned.1.call-update) | async-done | bytes 5242896 | tf_op jit(solution)/shard_map/all_gather | solution.py:147
  278.1 4.8 %fusion.37 = f32[8,4,40,128]{3,2,0,1:T(8,128)S(1)} fusion(bf16[8,4,40,2048]{3,2,0,1:T(8,128)(2,1)} %all-gather.15.cloned.1.call-done, bf16[4,2048,128]{2,1,0:T(8,128)(2,1)} %param.28), kind=kOutput, calls=%fused_computation.48 | convolution fusion | flops 671088640 | bytes 7995392 | tf_op jit(solution)/shard_map/secd,edf->secf/dot_general | solution.py:153
  283.4 2.3 fusion.46
  286.2 28.1 %all-gather.17.cloned.1.call-done = bf16[8,4,40,512]{3,2,0,1:T(8,128)(2,1)} async-done(((bf16[8,4,40,128]{3,2,0,1:T(8,128)(2,1)}), bf16[8,4,40,512]{3,2,0,1:T(8,128)(2,1)}) %all-gather.17.cloned.1.call-update) | async-done | bytes 1310736 | tf_op jit(solution)/shard_map/all_gather | solution.py:158
  314.4 2.2 fusion.31
  317.7 4.6 %all-to-all-start.1 = ((bf16[8,4,40,512]{3,2,1,0:T(8,128)(2,1)}), bf16[8,4,40,512]{3,2,1,0:T(8,128)(2,1)S(1)}, u32[]{:S(2)}, u32[]{:S(2)}) async-start(bf16[8,4,40,512]{3,2,1,0:T(8,128)(2,1)} %copy.62), calls=%async_computation.1 | async-start | bytes 2621440 | tf_op jit(solution)/shard_map/all_to_all | solution.py:162
  323.2 27.9 %all-gather.13.cloned.1.call-done = bf16[512,2048]{1,0:T(8,128)(2,1)} async-done(((bf16[512,512]{1,0:T(8,128)(2,1)}), bf16[512,2048]{1,0:T(8,128)(2,1)}) %all-gather.13.cloned.1.call-update) | async-done | bytes 2097168 | tf_op jit(solution)/shard_map/all_gather | solution.py:121
  351.1 2.5 fusion.62
  354.4 10.6 %all_gather.29 = bf16[512,512]{1,0:T(8,128)(2,1)} all-gather(bf16[512,128]{1,0:T(8,128)(2,1)S(1)} %fusion.49), channel_id=1, replica_groups=mesh['sp'=8,'tp'=4] {'tp'}, dimensions={1}, use_global_device_ids=true | all-gather | bytes 655360 | tf_op jit(solution)/shard_map/all_gather | solution.py:128
  365.0 5.1 %gather_fusion.1 = bf16[1024,512]{1,0:T(8,128)(2,1)} fusion(bf16[1280,512]{1,0:T(8,128)(2,1)S(1)} %bitcast.118, s32[1024]{0:T(1024)S(1)} %broadcast_clamp_fusion), kind=kCustom, calls=%fused_computation.1 | custom fusion | bytes 2101248 | tf_op jit(solution)/shard_map/gather | solution.py:164
  370.1 3.4 reshape.128
  373.5 4.5 %multiply_reduce_fusion = f32[512,512]{1,0:T(8,128)S(1)} fusion(f32[512,2,512]{2,1,0:T(2,128)} %reshape.128, f32[512,2]{1,0:T(8,128)S(1)} %copy-done.7), kind=kLoop, calls=%fused_computation.38 | loop fusion | flops 786432 | bytes 3149824 | tf_op jit(solution)/shard_map/reduce_sum | solution.py:165
  (107 shorter events, 15.9 us)
Async XLA Ops:
  6.5 307.8 %copy-start = (bf16[4,512,512]{2,1,0:T(8,128)(2,1)S(1)}, bf16[4,512,512]{2,1,0:T(8,128)(2,1)}, u32[]{:S(2)}) copy-start(bf16[4,512,512]{2,1,0:T(8,128)(2,1)} %param.30) | copy-start | bytes 6291460
  6.5 5.1 %copy-start.10 = (bf16[512,256]{1,0:T(8,128)(2,1)S(1)}, bf16[512,256]{1,0:T(8,128)(2,1)}, u32[]{:S(2)}) copy-start(bf16[512,256]{1,0:T(8,128)(2,1)} %param.19) | copy-start | bytes 786436
  6.5 5.2 %copy-start.9 = (f32[512,4]{0,1:T(4,128)S(1)}, f32[512,4]{0,1:T(4,128)}, u32[]{:S(2)}) copy-start(f32[512,4]{0,1:T(4,128)} %param.22) | copy-start | bytes 24580
  6.5 34.5 %all-gather.9.cloned.1.call-start = ((), (), s32[]{:S(2)}) async-start(), calls=%async_computation.3 | async-start | bytes 2359296 | tf_op jit(solution)/shard_map/all_gather | solution.py:64
  8.5 62.8 %all-gather.7.cloned.1.call-start = ((), (), s32[]{:S(2)}) async-start(), calls=%async_computation.2 | async-start | bytes 2359296 | tf_op jit(solution)/shard_map/all_gather | solution.py:63
  10.4 151.6 %all-gather.11.cloned.1.call-start = ((), (), s32[]{:S(2)}) async-start(), calls=%async_computation.4 | async-start | bytes 1310720 | tf_op jit(solution)/shard_map/all_gather | solution.py:108
  91.2 10.4 %copy-start.11 = (s32[512,2]{0,1:T(2,128)S(1)}, s32[512,2]{0,1:T(2,128)}, u32[]{:S(2)}) copy-start(s32[512,2]{0,1:T(2,128)} %param.26) | copy-start | bytes 12292
  92.1 186.0 %all-gather.15.cloned.1.call-start = ((), (), s32[]{:S(2)}) async-start(), calls=%async_computation.6 | async-start | bytes 6553600 | tf_op jit(solution)/shard_map/all_gather | solution.py:147
  166.8 9.2 %copy-start.5 = (bf16[512,512]{1,0:T(8,128)(2,1)}, bf16[512,512]{1,0:T(8,128)(2,1)S(1)}, u32[]{:S(2)}) copy-start(bf16[512,512]{1,0:T(8,128)(2,1)S(1)} %get-tuple-element.348) | copy-start | bytes 1572868
  176.0 4.8 %copy-start.2 = (bf16[512,512]{1,0:T(8,128)(2,1)}, bf16[512,512]{1,0:T(8,128)(2,1)S(1)}, u32[]{:S(2)}) copy-start(bf16[512,512]{1,0:T(8,128)(2,1)S(1)} %fusion.52) | copy-start | bytes 1572868
  218.8 95.6 %all-gather.17.cloned.1.call-start = ((), (), s32[]{:S(2)}) async-start(), calls=%async_computation.7 | async-start | bytes 1638400 | tf_op jit(solution)/shard_map/all_gather | solution.py:158
  278.1 4.8 %copy-start.1 = (bf16[8,4,40,2048]{3,2,0,1:T(8,128)(2,1)S(1)}, bf16[8,4,40,2048]{3,2,0,1:T(8,128)(2,1)}, u32[]{:S(2)}) copy-start(bf16[8,4,40,2048]{3,2,0,1:T(8,128)(2,1)} %all-gather.15.cloned.1.call-done) | copy-start | bytes 15728644
  278.1 5.3 %copy-start.13 = (bf16[4,2048,128]{2,1,0:T(8,128)(2,1)S(1)}, bf16[4,2048,128]{2,1,0:T(8,128)(2,1)}, u32[]{:S(2)}) copy-start(bf16[4,2048,128]{2,1,0:T(8,128)(2,1)} %param.29) | copy-start | bytes 6291460
  285.7 65.4 %all-gather.13.cloned.1.call-start = ((), (), s32[]{:S(2)}) async-start(), calls=%async_computation.5 | async-start | bytes 2621440 | tf_op jit(solution)/shard_map/all_gather | solution.py:121
  316.5 5.8 %copy-start.12 = (f32[512,2]{0,1:T(2,128)S(1)}, f32[512,2]{0,1:T(2,128)}, u32[]{:S(2)}) copy-start(f32[512,2]{0,1:T(2,128)} %param.27) | copy-start | bytes 12292
  317.7 47.3 %all-to-all-start.1 = ((bf16[8,4,40,512]{3,2,1,0:T(8,128)(2,1)}), bf16[8,4,40,512]{3,2,1,0:T(8,128)(2,1)S(1)}, u32[]{:S(2)}, u32[]{:S(2)}) async-start(bf16[8,4,40,512]{3,2,1,0:T(8,128)(2,1)} %copy.62), calls=%async_computation.1 | async-start | bytes 2621440 | tf_op jit(solution)/shard_map/all_to_all | solution.py:162
  351.1 2.5 copy-start.3
  351.1 2.5 copy-start.14
  370.1 3.4 copy-start.7
  373.5 4.5 %copy-start.4 = (bf16[512,512]{1,0:T(8,128)(2,1)S(1)}, bf16[512,512]{1,0:T(8,128)(2,1)}, u32[]{:S(2)}) copy-start(bf16[512,512]{1,0:T(8,128)(2,1)} %all_gather.29) | copy-start | bytes 1572868
  373.5 4.5 %copy-start.6 = (bf16[512,512]{1,0:T(8,128)(2,1)S(1)}, bf16[512,512]{1,0:T(8,128)(2,1)}, u32[]{:S(2)}) copy-start(bf16[512,512]{1,0:T(8,128)(2,1)} %copy-done.5) | copy-start | bytes 1572868
  373.5 4.6 %copy-start.8 = (bf16[512,512]{1,0:T(8,128)(2,1)S(1)}, bf16[512,512]{1,0:T(8,128)(2,1)}, u32[]{:S(2)}) copy-start(bf16[512,512]{1,0:T(8,128)(2,1)} %param.33) | copy-start | bytes 1572868
Sparse Core Ops, SparseCore 0:
  8.9 32.0 all-gather.8
  42.6 28.6 all-gather.6
  92.2 69.7 all-gather.10
  218.9 59.1 all-gather.14
  285.8 28.5 all-gather.16
  316.0 35.0 all-gather.12
